TPU v7x, 128 devices: a whole 4x4x4 slice. The times are simulated.
128 devices in a mesh: rep: 2 (over z_hi), fs: 32 (over z_lo, y, x), tp: 2 (over core).
Axes of the slice: x: 4, y: 4, z: 4 (z_hi: 2, z_lo: 2; z = z_hi * 2 + z_lo), core: 2. Of those that a mesh axis runs over, the one named last changes fastest.
Arguments:
- tokens: bfloat16 [65536, 2048], P(('rep', 'fs')), may hold values from -6 to 6
- norm_mix: bfloat16 [2048], replicated, may hold values from 0.099609375 to 1.8984375
- w_unit: bfloat16 [2048, 1024], P('fs', 'tp'), may hold values from -0.125 to 0.125
- w_value: bfloat16 [2048, 1024], P('fs', 'tp'), may hold values from -0.125 to 0.125
- spatial: bfloat16 [4, 128, 128], replicated, may hold values from -0.52734375 to 0.52734375
- spatial_bias: bfloat16 [4, 128], replicated, may hold values from 0.099609375 to 1.8984375
- group_gain: bfloat16 [1024], replicated, may hold values from 0.099609375 to 1.8984375
- group_shift: bfloat16 [1024], replicated, may hold values from -3 to 3
- w_mix_out: bfloat16 [1024, 2048], P('tp', 'fs'), may hold values from -0.1875 to 0.1875
- norm_ffn: bfloat16 [2048], replicated, may hold values from 0.099609375 to 1.8984375
- w_gate: bfloat16 [2048, 2816], P('fs', 'tp'), may hold values from -0.125 to 0.125
- w_up: bfloat16 [2048, 2816], P('fs', 'tp'), may hold values from -0.125 to 0.125
- w_down: bfloat16 [2816, 2048], P('tp', 'fs'), may hold values from -0.109375 to 0.109375
Outputs:
- layer_out: bfloat16 [65536, 2048], P(('rep', 'fs', 'tp'))
All inputs are finite; a program needn't handle non-finite values.
Results may differ from a plain program's by a relative error of at most 0.008.
Values may be sent and summed in bfloat16 or wider, within the bound.
No kernel may reach another device: no remote copies, remote signals or barrier semaphores. Data moves between devices by JAX's collectives and lax.ppermute only.
A program may use at most 128 MiB of HBM per device.

v0:
```python
import jax
import jax.numpy as jnp
from jax import lax
from jax.sharding import PartitionSpec as P


def sent_together(arrays, axis, dim, along):
    ends, at = ([], 0)
    for a in arrays[:-1]:
        at += a.shape[along]
        ends.append(at)
    both = jnp.concatenate(arrays, axis=along)
    return tuple(jnp.split(lax.all_gather(both, axis, axis=dim, tiled=True), ends, axis=along))


def sent_to_all(x, axis):
    copies = jnp.broadcast_to(x, (lax.axis_size(axis), *x.shape))
    return lax.all_to_all(copies, axis, split_axis=0, concat_axis=0, tiled=True)


def in_order(pieces, dim):
    pieces = jnp.moveaxis(pieces, 0, dim)
    dims = pieces.shape
    return pieces.reshape(*dims[:dim], dims[dim] * dims[dim + 1], *dims[dim + 2 :])


def gathered_copies(x, axis, dim):
    pieces = sent_to_all(x, axis)
    return in_order(pieces, dim)


def total_of_pieces(x, axis):
    return lax.all_gather(x, axis).sum(0)


def split_up(x, dim, peers):
    before, after = (x.shape[:dim], x.shape[dim + 1 :])
    return jnp.moveaxis(x.reshape(*before, peers, -1, *after), dim, 0)


def summed_on_arrival(x, axis, dim):
    pieces = split_up(x, dim, lax.axis_size(axis))
    arrived = lax.all_to_all(pieces, axis, split_axis=0, concat_axis=0, tiled=True)
    return arrived.astype(jnp.float32).sum(axis=0)


def rms_scale(values, gain):
    values = values.astype(jnp.float32)
    scale = lax.rsqrt(jnp.mean(values * values, axis=-1, keepdims=True) + 1e-06)
    return values * scale * gain.astype(jnp.float32)


def spatial_unit(unit_pre, value_pre, spatial, spatial_bias, group_gain, group_shift):
    count, width = value_pre.shape
    groups = spatial.shape[0]
    block = spatial.shape[1]
    active = jax.nn.gelu(value_pre, approximate=True).reshape(count, groups, width // groups)
    center = jnp.mean(active, axis=-1, keepdims=True)
    spread = jnp.mean(jnp.square(active - center), axis=-1, keepdims=True)
    normal = ((active - center) * lax.rsqrt(spread + 1e-06)).reshape(count, width)
    normal = normal * group_gain.astype(jnp.float32) + group_shift.astype(jnp.float32)
    grouped = normal.astype(jnp.bfloat16)
    causal = jnp.tril(jnp.ones((block, block), dtype=bool))
    weights = jnp.where(causal[None], spatial, jnp.zeros_like(spatial))
    tiles = grouped.reshape(count // block, block, groups, width // groups)
    mixed = jnp.einsum("gts,nsgd->ntgd", weights, tiles, preferred_element_type=jnp.float32)
    mixed = mixed + spatial_bias.astype(jnp.float32).T[None, :, :, None]
    return jax.nn.gelu(unit_pre, approximate=True) * mixed.reshape(count, width)


def on_device(
    tokens,
    norm_mix,
    w_unit,
    w_value,
    spatial,
    spatial_bias,
    group_gain,
    group_shift,
    w_mix_out,
    norm_ffn,
    w_gate,
    w_up,
    w_down,
):
    count = tokens.shape[0]
    half = count // lax.axis_size("tp")
    position = lax.axis_index("tp")
    row_start = position * half
    local_width = w_unit.shape[1]
    group_count = spatial.shape[0] // lax.axis_size("tp")
    group_start = position * group_count
    spatial_local = lax.dynamic_slice_in_dim(spatial, group_start, group_count, 0)
    bias_local = lax.dynamic_slice_in_dim(spatial_bias, group_start, group_count, 0)
    gain_local = lax.dynamic_slice_in_dim(group_gain, position * local_width, local_width, 0)
    shift_local = lax.dynamic_slice_in_dim(group_shift, position * local_width, local_width, 0)
    normed = rms_scale(tokens, norm_mix).astype(jnp.bfloat16)
    unit_whole, value_whole = sent_together((w_unit, w_value), "fs", 0, 1)
    unit_pre = jnp.dot(normed, unit_whole, preferred_element_type=jnp.float32)
    value_pre = jnp.dot(normed, value_whole, preferred_element_type=jnp.float32)
    gated = spatial_unit(
        unit_pre, value_pre, spatial_local, bias_local, gain_local, shift_local
    ).astype(jnp.bfloat16)
    partial_terms = jnp.dot(
        gated, gathered_copies(w_mix_out, "fs", 1), preferred_element_type=jnp.float32
    )
    summed = total_of_pieces(partial_terms, "tp")
    h_mid = (tokens.astype(jnp.float32) + summed).astype(jnp.bfloat16)
    normed_mid = rms_scale(h_mid, norm_ffn).astype(jnp.bfloat16)
    gate_whole, up_whole = sent_together((w_gate, w_up), "fs", 0, 1)
    gate = jnp.dot(normed_mid, gate_whole, preferred_element_type=jnp.float32)
    up = jnp.dot(normed_mid, up_whole, preferred_element_type=jnp.float32)
    hidden = (jax.nn.silu(gate) * up).astype(jnp.bfloat16)
    down_cols = lax.all_gather(w_down, "fs", axis=1, tiled=True)
    residual_rows = lax.dynamic_slice_in_dim(h_mid, row_start, half, 0).astype(jnp.float32)
    summed_rows = summed_on_arrival(
        jnp.dot(hidden, down_cols, preferred_element_type=jnp.float32).astype(jnp.bfloat16), "tp", 0
    )
    return (residual_rows + summed_rows).astype(jnp.bfloat16)


def solution(mesh):
    placed = (
        P(("rep", "fs"), None),
        P(),
        P("fs", "tp"),
        P("fs", "tp"),
        P(),
        P(),
        P(),
        P(),
        P("tp", "fs"),
        P(),
        P("fs", "tp"),
        P("fs", "tp"),
        P("tp", "fs"),
    )
    return jax.shard_map(
        on_device,
        mesh=mesh,
        in_specs=placed,
        out_specs=P(("rep", "fs", "tp"), None),
        check_vma=False,
    )
```

profile of v0, /device:TPU:1, one launch (start us, length us, event | category | flops | bytes accessed | tf_op | source)
XLA Modules:
  0.0 629.2 jit_solution(16438548954573870074)
XLA Ops:
  6.5 0.0 all-gather.6.cloned.1.call-start
  6.6 1.6 pad_maximum_fusion.1
  8.1 0.0 all-gather.6.cloned.1.call-update
  8.2 2.4 broadcast_in_dim.13
  10.6 9.3 %all-to-all-start = ((bf16[32,512,64]{1,2,0:T(8,128)(2,1)}), bf16[32,512,64]{1,2,0:T(8,128)(2,1)}, u32[]{:S(2)}, u32[]{:S(2)}) async-start(bf16[32,512,64]{1,2,0:T(8,128)(2,1)} %broadcast_in_dim.13), calls=%async_computation | async-start | bytes 4194304 | tf_op jit(solution)/shard_map/all_to_all | solution.py:18
  19.9 0.0 all-gather.12.cloned.1.call-start
  20.0 0.0 copy-done.5
  20.0 0.0 copy-done.9
  20.0 0.0 copy-done.8
  20.0 0.1 dynamic-slice_convert_fusion
  20.1 3.1 fusion.3
  23.3 133.9 %all-gather.6.cloned.1.call-done = bf16[2048,1024]{1,0:T(8,128)(2,1)} async-done(((bf16[64,1024]{1,0:T(8,128)(2,1)}), bf16[2048,1024]{1,0:T(8,128)(2,1)}) %all-gather.6.cloned.1.call-update) | async-done | bytes 4194320 | tf_op jit(solution)/shard_map/all_gather | solution.py:13
  157.1 6.9 %fusion.35 = f32[1024,512]{1,0:T(8,128)} fusion(bf16[2048,1024]{1,0:T(8,128)(2,1)} %all-gather.6.cloned.1.call-done, bf16[1024,2048]{1,0:T(8,128)(2,1)} %param.13, f32[2048]{0:T(1024)S(1)} %convert_element_type.51, f32[1024]{0:T(1024)S(1)} %add_rsqrt_fusion.2), kind=kOutput, calls=%fused_computation.39 | convolution fusion | flops 2160066560 | bytes 8400896 | tf_op jit(solution)/shard_map/dot_general | solution.py:100
  164.1 2.6 reshape.58
  166.7 1.2 reduce_sum.55
  167.9 14.4 %multiply_reduce_fusion = f32[1024,2]{1,0:T(8,128)S(1)} fusion(f32[1024,2,256]{2,1,0:T(2,128)S(1)} %reshape.58, f32[1024,2]{1,0:T(8,128)S(1)} %broadcast_multiply_fusion), kind=kLoop, calls=%fused_computation.46 | loop fusion | flops 1570816 | bytes 2113536 | tf_op jit(solution)/shard_map/reduce_sum | solution.py:59
  182.3 0.1 add_rsqrt_fusion
  182.4 1.2 mul.112
  183.6 0.2 copy.32
  183.8 1.2 sub.17
  185.1 0.2 copy.31
  185.3 0.2 copy-done.1
  185.4 0.8 add_convert_fusion.1
  186.2 0.3 reshape.59
  186.5 0.5 bitcast_add_fusion
  187.1 2.4 copy.28
  189.5 1.8 copy.33
  191.2 0.0 all-to-all-done
  191.3 11.6 %fusion.51 = f32[1024,2048]{1,0:T(8,128)} fusion(bf16[512,2048]{0,1:T(8,128)(2,1)} %bitcast.5, f32[1024,512]{1,0:T(8,128)S(1)} %bitcast.30, bf16[2048,1024]{1,0:T(8,128)(2,1)} %all-gather.6.cloned.1.call-done, bf16[1024,2048]{1,0:T(8,128)(2,1)} %param.13, f32[2048]{0:T(1024)S(1)} %convert_element_type.51, f32[1024]{0:T(1024)S(1)} %add_rsqrt_fusion.2), kind=kOutput, calls=%fused_computation.47 | convolution fusion | flops 4308598784 | bytes 18886656 | tf_op jit(solution)/shard_map/dot_general | solution.py:104
  202.9 0.0 all-gather.12.cloned.1.call-update
  202.9 0.0 all-gather.8.cloned.1.call-start
  203.0 0.8 copy-done.2
  203.8 0.1 copy-done.3
  203.9 0.8 pad_maximum_fusion
  204.6 0.0 all-gather.8.cloned.1.call-update
  204.7 0.0 all-gather.10.cloned.1.call-start
  204.7 0.5 all-gather.10.cloned.1.call-update
  205.3 49.1 %all-gather.12.cloned.1.call-done = f32[2048,2048]{1,0:T(8,128)} async-done(((f32[1024,2048]{1,0:T(8,128)}), f32[2048,2048]{1,0:T(8,128)}) %all-gather.12.cloned.1.call-update) | async-done | bytes 16777232 | tf_op jit(solution)/shard_map/all_gather | solution.py:33
  254.4 11.8 %reduce_sum.57 = f32[1024,2048]{1,0:T(8,128)} reduce(f32[2,1024,2048]{2,1,0:T(8,128)} %bitcast.23, f32[]{:T(128)} %constant.15.clone.1), dimensions={0}, to_apply=%region_3.4 | reduce | flops 2097152 | bytes 25165828 | tf_op jit(solution)/shard_map/reduce_sum | solution.py:33
  266.1 7.8 %fusion = (f32[1024]{0:T(1024)S(1)}, bf16[1024,2048]{1,0:T(8,128)(2,1)}) fusion(f32[1024,2048]{1,0:T(8,128)} %reduce_sum.57, bf16[1024,2048]{1,0:T(8,128)(2,1)} %param.13), kind=kLoop, calls=%fused_computation.5 | loop fusion | flops 12581888 | bytes 16781312 | tf_op jit(solution)/shard_map/reduce_sum | solution.py:49
  273.9 135.7 %all-gather.8.cloned.1.call-done = bf16[2048,2816]{1,0:T(8,128)(2,1)} async-done(((bf16[64,2816]{1,0:T(8,128)(2,1)}), bf16[2048,2816]{1,0:T(8,128)(2,1)}) %all-gather.8.cloned.1.call-update) | async-done | bytes 11534352 | tf_op jit(solution)/shard_map/all_gather | solution.py:13
  409.6 11.9 %fusion.9 = f32[1024,1408]{1,0:T(8,128)} fusion(bf16[2048,2816]{1,0:T(8,128)(2,1)} %all-gather.8.cloned.1.call-done, bf16[1024,2048]{1,0:T(8,128)(2,1)} %get-tuple-element.6, f32[2048]{0:T(1024)S(1)} %convert_element_type.60, f32[1024]{0:T(1024)S(1)} %add_rsqrt_fusion.1), kind=kOutput, calls=%fused_computation.15 | convolution fusion | flops 5913968640 | bytes 15740928 | tf_op jit(solution)/shard_map/dot_general | solution.py:111
  421.5 147.9 %all-gather.10.cloned.1.call-done = bf16[1408,2048]{0,1:T(8,128)(2,1)} async-done(((bf16[1408,64]{0,1:T(8,128)(2,1)}), bf16[1408,2048]{0,1:T(8,128)(2,1)}) %all-gather.10.cloned.1.call-update) | async-done | bytes 5767184 | tf_op jit(solution)/shard_map/all_gather | solution.py:114
  569.4 20.9 %fusion.16 = bf16[1024,2048]{1,0:T(8,128)(2,1)} fusion(bf16[1408,2048]{0,1:T(8,128)(2,1)} %all-gather.10.cloned.1.call-done, f32[1024,1408]{1,0:T(8,128)} %fusion.9, bf16[2048,2816]{1,0:T(8,128)(2,1)} %all-gather.8.cloned.1.call-done, bf16[1024,2048]{1,0:T(8,128)(2,1)} %get-tuple-element.6, f32[2048]{0:T(1024)S(1)} %convert_element_type.60, ...), kind=kOutput, calls=%fused_computation.20 | convolution fusion | flops 11830296576 | bytes 25702400 | tf_op jit(solution)/shard_map/dot_general | solution.py:117
  590.3 28.2 %all_to_all.10 = bf16[2,512,2048]{2,1,0:T(8,128)(2,1)S(1)} all-to-all(bf16[2,512,2048]{2,1,0:T(8,128)(2,1)} %bitcast.29), channel_id=1, replica_groups=mesh['rep'=2,'fs'=32,'tp'=2] {'tp'}, dimensions={0} | all-to-all | bytes 8388608 | tf_op jit(solution)/shard_map/all_to_all | solution.py:43
  618.5 1.0 convert_reduce_fusion
  619.4 1.2 copy-done
  620.7 2.1 add_convert_fusion
  (20 shorter events, 0.1 us)
Async XLA Ops:
  6.5 13.4 %copy-start.5 = (bf16[2048]{0:T(1024)(128)(2,1)S(1)}, bf16[2048]{0:T(1024)(128)(2,1)}, u32[]{:S(2)}) copy-start(bf16[2048]{0:T(1024)(128)(2,1)} %param.14) | copy-start | bytes 12292
  6.5 13.5 %copy-start.9 = (bf16[4,128]{1,0:T(4,128)(2,1)S(1)}, bf16[4,128]{1,0:T(4,128)(2,1)}, u32[]{:S(2)}) copy-start(bf16[4,128]{1,0:T(4,128)(2,1)} %param.18) | copy-start | bytes 3076
  6.5 13.5 %copy-start.8 = (bf16[1024]{0:T(1024)(128)(2,1)S(1)}, bf16[1024]{0:T(1024)(128)(2,1)}, u32[]{:S(2)}) copy-start(bf16[1024]{0:T(1024)(128)(2,1)} %param.19) | copy-start | bytes 6148
  6.5 13.5 %copy-start.7 = (bf16[1024]{0:T(1024)(128)(2,1)S(1)}, bf16[1024]{0:T(1024)(128)(2,1)}, u32[]{:S(2)}) copy-start(bf16[1024]{0:T(1024)(128)(2,1)} %param.20) | copy-start | bytes 6148
  6.5 150.6 %all-gather.6.cloned.1.call-start = ((), (), s32[]{:S(2)}) async-start(), calls=%async_computation.2 | async-start | bytes 4325376 | tf_op jit(solution)/shard_map/all_gather | solution.py:13
  10.6 180.7 %all-to-all-start = ((bf16[32,512,64]{1,2,0:T(8,128)(2,1)}), bf16[32,512,64]{1,2,0:T(8,128)(2,1)}, u32[]{:S(2)}, u32[]{:S(2)}) async-start(bf16[32,512,64]{1,2,0:T(8,128)(2,1)} %broadcast_in_dim.13), calls=%async_computation | async-start | bytes 4194304 | tf_op jit(solution)/shard_map/all_to_all | solution.py:18
  19.9 234.4 %all-gather.12.cloned.1.call-start = ((), (), s32[]{:S(2)}) async-start(), calls=%async_computation.5 | async-start | bytes 25165824 | tf_op jit(solution)/shard_map/all_gather | solution.py:33
  183.8 1.6 copy-start.1
  185.4 1.1 copy-start.4
  202.9 0.9 copy-start.2
  202.9 1.0 copy-start.3
  202.9 2.4 copy-start.6
  202.9 206.7 %all-gather.8.cloned.1.call-start = ((), (), s32[]{:S(2)}) async-start(), calls=%async_computation.3 | async-start | bytes 11894784 | tf_op jit(solution)/shard_map/all_gather | solution.py:13
  204.7 364.7 %all-gather.10.cloned.1.call-start = ((), (), s32[]{:S(2)}) async-start(), calls=%async_computation.4 | async-start | bytes 5947392 | tf_op jit(solution)/shard_map/all_gather | solution.py:114
  618.5 2.2 copy-start
Sparse Core Ops, SparseCore 0:
  9.0 148.1 all-gather.5
  203.0 51.2 all-gather.11
  256.0 153.5 all-gather.7
  411.1 158.2 all-gather.9
where the time goes:
time: 630 us; the launch traced here: 629 us
  waiting for transfers between devices  467 us (74%)
  matrix products  51.8 us (8%)
  other arithmetic  44.6 us (7%)
  blocking collectives  28.2 us (4%)
  local copies, waits for them, and re-layouts  14.5 us (2%)
  between operations  13.3 us (2%)
  starting transfers between devices  9.5 us (2%)
    all_gather x2, waiting for transfers between devices, sent_together(): lax.all_gather(both, axis, axis=dim, tiled=True)  270 us
    all_gather x1, waiting for transfers between devices, on_device(): down_cols = lax.all_gather(w_down, 'fs', axis=1, tiled=True)  148 us
    all_gather x1, waiting for transfers between devices, total_of_pieces(): return lax.all_gather(x, axis).sum(0)  49.1 us
    all_to_all x1, blocking collectives, summed_on_arrival(): lax.all_to_all(pieces, axis, split_axis=0, concat_axis=0, tiled=True)  28.2 us
    dot_general x1, matrix products, on_device(): jnp.dot(hidden, down_cols, preferred_element_type=jnp.float32)  20.9 us
    reduce_sum x1, other arithmetic, spatial_unit(): spread = jnp.mean(jnp.square(active - center), axis=-1, keepdims=True)  14.4 us
  transfers between devices with their start and end apart: 5, of which 4 were waited for; matrix products, arithmetic and copies ran while one was open for 11% of the time, Pallas kernels for 0%

commit v1 on v0

--- a/solution.py
+++ b/solution.py
@@ -111,7 +111,10 @@
     gate = jnp.dot(normed_mid, gate_whole, preferred_element_type=jnp.float32)
     up = jnp.dot(normed_mid, up_whole, preferred_element_type=jnp.float32)
     hidden = (jax.nn.silu(gate) * up).astype(jnp.bfloat16)
-    down_cols = lax.all_gather(w_down, "fs", axis=1, tiled=True)
+    wide_out = jnp.stack([w_down for _ in range(jax.lax.psum(1, axis_name="fs"))])
+    down_cols = jnp.concatenate(
+        jax.lax.all_to_all(wide_out, "fs", split_axis=0, concat_axis=0), axis=1
+    )
     residual_rows = lax.dynamic_slice_in_dim(h_mid, row_start, half, 0).astype(jnp.float32)
     summed_rows = summed_on_arrival(
         jnp.dot(hidden, down_cols, preferred_element_type=jnp.float32).astype(jnp.bfloat16), "tp", 0

time: 630 us -> 497 us (0.79)
  waiting for transfers between devices: 467 us -> 330 us
    all_gather x1 -> x0, waiting for transfers between devices: 148 us -> none  [on_device(): down_cols = lax.all_gather(w_down, 'fs', axis=1, tiled=True)]
    all_gather x2, waiting for transfers between devices: 270 us -> 288 us  [sent_together(): lax.all_gather(both, axis, axis=dim, tiled=True)]
    all_gather x1, waiting for transfers between devices: 49.1 us -> 41.4 us  [total_of_pieces(): return lax.all_gather(x, axis).sum(0)]
  transfers between devices with their start and end apart: 5 -> 5, of which waited for: 4 -> 3; matrix products, arithmetic and copies ran while one was open for 11% -> 15% of each run, Pallas kernels for 0% -> 0%
where the time goes in v1:
time: 497 us
  waiting for transfers between devices  330 us (66%)
  matrix products  51.9 us (10%)
  other arithmetic  44.6 us (9%)
  blocking collectives  25 us (5%)
  local copies, waits for them, and re-layouts  17.8 us (4%)
  starting transfers between devices  14.5 us (3%)
  between operations  13.3 us (3%)
    all_gather x2, waiting for transfers between devices, sent_together(): lax.all_gather(both, axis, axis=dim, tiled=True)  288 us
    all_gather x1, waiting for transfers between devices, total_of_pieces(): return lax.all_gather(x, axis).sum(0)  41.4 us
    all_to_all x1, blocking collectives, summed_on_arrival(): lax.all_to_all(pieces, axis, split_axis=0, concat_axis=0, tiled=True)  25 us
    dot_general x1, matrix products, on_device(): jnp.dot(hidden, down_cols, preferred_element_type=jnp.float32)  20.9 us
    reduce_sum x1, other arithmetic, spatial_unit(): spread = jnp.mean(jnp.square(active - center), axis=-1, keepdims=True)  14.4 us
    dot_general x1, matrix products, on_device(): gate = jnp.dot(normed_mid, gate_whole, preferred_element_type=jnp.float32)  11.9 us
    reduce_sum x1, other arithmetic, total_of_pieces(): return lax.all_gather(x, axis).sum(0)  11.8 us
    dot_general x1, matrix products, on_device(): jnp.dot(gated, gathered_copies(w_mix_out, 'fs', 1), preferred_element_typ...  11.6 us
  transfers between devices with their start and end apart: 5, of which 3 were waited for; matrix products, arithmetic and copies ran while one was open for 15% of the time, Pallas kernels for 0%

profile of v1, /device:TPU:1, one launch (start us, length us, event | category | flops | bytes accessed | tf_op | source)
XLA Modules:
  0.0 496.8 jit_solution(9141011168080807351)
XLA Ops:
  6.5 0.0 all-gather.5.cloned.1.call-start
  6.6 1.6 pad_maximum_fusion.1
  8.1 0.0 all-gather.5.cloned.1.call-update
  8.2 2.4 broadcast_in_dim.13
  10.6 9.3 %all-to-all-start = ((bf16[32,512,64]{1,2,0:T(8,128)(2,1)}), bf16[32,512,64]{1,2,0:T(8,128)(2,1)}, u32[]{:S(2)}, u32[]{:S(2)}) async-start(bf16[32,512,64]{1,2,0:T(8,128)(2,1)} %broadcast_in_dim.13), calls=%async_computation | async-start | bytes 4194304 | tf_op jit(solution)/shard_map/all_to_all | solution.py:18
  19.9 0.0 all-gather.9.cloned.1.call-start
  20.0 0.0 copy-done.6
  20.0 0.0 copy-done.10
  20.0 0.1 dynamic-slice_convert_fusion
  20.1 3.1 fusion.3
  23.3 133.9 %all-gather.5.cloned.1.call-done = bf16[2048,1024]{1,0:T(8,128)(2,1)} async-done(((bf16[64,1024]{1,0:T(8,128)(2,1)}), bf16[2048,1024]{1,0:T(8,128)(2,1)}) %all-gather.5.cloned.1.call-update) | async-done | bytes 4194320 | tf_op jit(solution)/shard_map/all_gather | solution.py:13
  157.1 6.9 %fusion.35 = f32[1024,512]{1,0:T(8,128)} fusion(bf16[2048,1024]{1,0:T(8,128)(2,1)} %all-gather.5.cloned.1.call-done, bf16[1024,2048]{1,0:T(8,128)(2,1)} %param.13, f32[2048]{0:T(1024)S(1)} %convert_element_type.51, f32[1024]{0:T(1024)S(1)} %add_rsqrt_fusion.2), kind=kOutput, calls=%fused_computation.39 | convolution fusion | flops 2160066560 | bytes 8400896 | tf_op jit(solution)/shard_map/dot_general | solution.py:100
  164.1 2.6 reshape.66
  166.7 1.2 reduce_sum.55
  167.9 14.4 %multiply_reduce_fusion = f32[1024,2]{1,0:T(8,128)S(1)} fusion(f32[1024,2,256]{2,1,0:T(2,128)S(1)} %reshape.66, f32[1024,2]{1,0:T(8,128)S(1)} %broadcast_multiply_fusion), kind=kLoop, calls=%fused_computation.46 | loop fusion | flops 1570816 | bytes 2113536 | tf_op jit(solution)/shard_map/reduce_sum | solution.py:59
  182.3 0.1 add_rsqrt_fusion
  182.4 1.2 mul.112
  183.6 0.2 copy.33
  183.8 1.2 sub.17
  185.1 0.2 copy.32
  185.3 0.2 copy-done.1
  185.4 0.8 add_convert_fusion.1
  186.2 0.3 reshape.67
  186.5 0.5 bitcast_add_fusion
  187.1 2.4 copy.29
  189.5 1.8 copy.34
  191.2 0.0 all-to-all-done
  191.3 11.6 %fusion.51 = f32[1024,2048]{1,0:T(8,128)} fusion(bf16[512,2048]{0,1:T(8,128)(2,1)} %bitcast.5, f32[1024,512]{1,0:T(8,128)S(1)} %bitcast.33, bf16[2048,1024]{1,0:T(8,128)(2,1)} %all-gather.5.cloned.1.call-done, bf16[1024,2048]{1,0:T(8,128)(2,1)} %param.13, f32[2048]{0:T(1024)S(1)} %convert_element_type.51, f32[1024]{0:T(1024)S(1)} %add_rsqrt_fusion.2), kind=kOutput, calls=%fused_computation.47 | convolution fusion | flops 4308598784 | bytes 18886656 | tf_op jit(solution)/shard_map/dot_general | solution.py:104
  202.9 0.0 all-gather.9.cloned.1.call-update
  202.9 0.0 all-gather.7.cloned.1.call-start
  203.0 0.8 copy-done.3
  203.8 0.1 copy-done.4
  203.9 0.8 pad_maximum_fusion
  204.6 0.0 all-gather.7.cloned.1.call-update
  204.7 3.3 stack.2
  207.9 5.0 %all-to-all-start.1 = ((bf16[32,1408,64]{1,2,0:T(8,128)(2,1)}), bf16[32,1408,64]{1,2,0:T(8,128)(2,1)}, u32[]{:S(2)}, u32[]{:S(2)}) async-start(bf16[32,1408,64]{1,2,0:T(8,128)(2,1)} %stack.2), calls=%async_computation.1 | async-start | bytes 11534336 | tf_op jit(solution)/shard_map/all_to_all | solution.py:116
  213.0 0.0 copy-done.7
  213.0 41.4 %all-gather.9.cloned.1.call-done = f32[2048,2048]{1,0:T(8,128)} async-done(((f32[1024,2048]{1,0:T(8,128)}), f32[2048,2048]{1,0:T(8,128)}) %all-gather.9.cloned.1.call-update) | async-done | bytes 16777232 | tf_op jit(solution)/shard_map/all_gather | solution.py:33
  254.4 11.8 %reduce_sum.57 = f32[1024,2048]{1,0:T(8,128)} reduce(f32[2,1024,2048]{2,1,0:T(8,128)} %bitcast.26, f32[]{:T(128)} %constant.15.clone.1), dimensions={0}, to_apply=%region_3.4 | reduce | flops 2097152 | bytes 25165828 | tf_op jit(solution)/shard_map/reduce_sum | solution.py:33
  266.1 7.7 %fusion = (f32[1024]{0:T(1024)S(1)}, bf16[1024,2048]{1,0:T(8,128)(2,1)}) fusion(f32[1024,2048]{1,0:T(8,128)} %reduce_sum.57, bf16[1024,2048]{1,0:T(8,128)(2,1)} %param.13), kind=kLoop, calls=%fused_computation.5 | loop fusion | flops 12581888 | bytes 16781312 | tf_op jit(solution)/shard_map/reduce_sum | solution.py:49
  273.8 154.4 %all-gather.7.cloned.1.call-done = bf16[2048,2816]{1,0:T(8,128)(2,1)} async-done(((bf16[64,2816]{1,0:T(8,128)(2,1)}), bf16[2048,2816]{1,0:T(8,128)(2,1)}) %all-gather.7.cloned.1.call-update) | async-done | bytes 11534352 | tf_op jit(solution)/shard_map/all_gather | solution.py:13
  428.2 11.9 %fusion.9 = f32[1024,1408]{1,0:T(8,128)} fusion(bf16[2048,2816]{1,0:T(8,128)(2,1)} %all-gather.7.cloned.1.call-done, bf16[1024,2048]{1,0:T(8,128)(2,1)} %get-tuple-element.6, f32[2048]{0:T(1024)S(1)} %convert_element_type.60, f32[1024]{0:T(1024)S(1)} %add_rsqrt_fusion.1), kind=kOutput, calls=%fused_computation.15 | convolution fusion | flops 5913968640 | bytes 15740928 | tf_op jit(solution)/shard_map/dot_general | solution.py:111
  440.1 0.0 all-to-all-done.1
  440.1 20.9 %fusion.16 = bf16[1024,2048]{1,0:T(8,128)(2,1)} fusion(bf16[1408,2048]{0,1:T(8,128)(2,1)} %bitcast.8, f32[1024,1408]{1,0:T(8,128)} %fusion.9, bf16[2048,2816]{1,0:T(8,128)(2,1)} %all-gather.7.cloned.1.call-done, bf16[1024,2048]{1,0:T(8,128)(2,1)} %get-tuple-element.6, f32[2048]{0:T(1024)S(1)} %convert_element_type.60, f32[1024]{0:T(1024)S(1)} %add_rsqrt_fusion.1), kind=kOutput, calls=%fused_computation.20 | convolution fusion | flops 11830296576 | bytes 25702400 | tf_op jit(solution)/shard_map/dot_general | solution.py:120
  461.0 25.0 %all_to_all.15 = bf16[2,512,2048]{2,1,0:T(8,128)(2,1)S(1)} all-to-all(bf16[2,512,2048]{2,1,0:T(8,128)(2,1)} %bitcast.32), channel_id=1, replica_groups=mesh['rep'=2,'fs'=32,'tp'=2] {'tp'}, dimensions={0} | all-to-all | bytes 8388608 | tf_op jit(solution)/shard_map/all_to_all | solution.py:43
  486.0 1.0 convert_reduce_fusion
  487.0 1.2 copy-done
  488.2 2.1 add_convert_fusion
  (22 shorter events, 0.1 us)
Async XLA Ops:
  6.5 13.4 %copy-start.6 = (bf16[2048]{0:T(1024)(128)(2,1)S(1)}, bf16[2048]{0:T(1024)(128)(2,1)}, u32[]{:S(2)}) copy-start(bf16[2048]{0:T(1024)(128)(2,1)} %param.14) | copy-start | bytes 12292
  6.5 13.5 %copy-start.10 = (bf16[4,128]{1,0:T(4,128)(2,1)S(1)}, bf16[4,128]{1,0:T(4,128)(2,1)}, u32[]{:S(2)}) copy-start(bf16[4,128]{1,0:T(4,128)(2,1)} %param.18) | copy-start | bytes 3076
  6.5 13.5 %copy-start.9 = (bf16[1024]{0:T(1024)(128)(2,1)S(1)}, bf16[1024]{0:T(1024)(128)(2,1)}, u32[]{:S(2)}) copy-start(bf16[1024]{0:T(1024)(128)(2,1)} %param.19) | copy-start | bytes 6148
  6.5 13.5 %copy-start.8 = (bf16[1024]{0:T(1024)(128)(2,1)S(1)}, bf16[1024]{0:T(1024)(128)(2,1)}, u32[]{:S(2)}) copy-start(bf16[1024]{0:T(1024)(128)(2,1)} %param.20) | copy-start | bytes 6148
  6.5 150.6 %all-gather.5.cloned.1.call-start = ((), (), s32[]{:S(2)}) async-start(), calls=%async_computation.3 | async-start | bytes 4325376 | tf_op jit(solution)/shard_map/all_gather | solution.py:13
  10.6 180.7 %all-to-all-start = ((bf16[32,512,64]{1,2,0:T(8,128)(2,1)}), bf16[32,512,64]{1,2,0:T(8,128)(2,1)}, u32[]{:S(2)}, u32[]{:S(2)}) async-start(bf16[32,512,64]{1,2,0:T(8,128)(2,1)} %broadcast_in_dim.13), calls=%async_computation | async-start | bytes 4194304 | tf_op jit(solution)/shard_map/all_to_all | solution.py:18
  19.9 234.4 %all-gather.9.cloned.1.call-start = ((), (), s32[]{:S(2)}) async-start(), calls=%async_computation.5 | async-start | bytes 25165824 | tf_op jit(solution)/shard_map/all_gather | solution.py:33
  183.8 1.6 copy-start.1
  185.4 1.1 copy-start.5
  202.9 0.9 copy-start.3
  202.9 1.0 copy-start.4
  202.9 1.8 copy-start.2
  202.9 225.3 %all-gather.7.cloned.1.call-start = ((), (), s32[]{:S(2)}) async-start(), calls=%async_computation.4 | async-start | bytes 11894784 | tf_op jit(solution)/shard_map/all_gather | solution.py:13
  207.9 5.0 %copy-start.7 = (bf16[2048]{0:T(1024)(128)(2,1)S(1)}, bf16[2048]{0:T(1024)(128)(2,1)}, u32[]{:S(2)}) copy-start(bf16[2048]{0:T(1024)(128)(2,1)} %param.22) | copy-start | bytes 12292
  207.9 232.2 %all-to-all-start.1 = ((bf16[32,1408,64]{1,2,0:T(8,128)(2,1)}), bf16[32,1408,64]{1,2,0:T(8,128)(2,1)}, u32[]{:S(2)}, u32[]{:S(2)}) async-start(bf16[32,1408,64]{1,2,0:T(8,128)(2,1)} %stack.2), calls=%async_computation.1 | async-start | bytes 11534336 | tf_op jit(solution)/shard_map/all_to_all | solution.py:116
  486.0 2.2 copy-start
Sparse Core Ops, SparseCore 0:
  9.0 148.1 all-gather.4
  203.0 51.2 all-gather.8
  256.0 172.1 all-gather.6
